TPU v7x, 32 devices: a whole 2x2x4 slice. The times are simulated.
32 devices in a mesh: fs: 8 (over z, x), tp: 4 (over y, core).
Axes of the slice: x: 2, y: 2, z: 4, core: 2. Of those that a mesh axis runs over, the one named last changes fastest.
Arguments:
- tokens: bfloat16 [3072, 4096], P('fs', 'tp'), may hold values from -600 to 600
- gate_master: float32 [8, 4096, 512], P(None, 'fs', 'tp'), may hold values from -0.09375 to 0.09375
- up_master: float32 [8, 4096, 512], P(None, 'fs', 'tp'), may hold values from -0.09375 to 0.09375
- down_master: float32 [8, 4096, 512], P(None, 'fs', 'tp'), may hold values from -0.25 to 0.25
- norm_gain: float32 [4096], P('fs'), may hold values from 0.1 to 1.9
- routes: int32 [3072, 2], P('fs'), may hold values from 0 to 7, all different within a row; in each aligned block of 384 rows (0 to 383, 384 to 767, ...) at most 192 rows name the same one
- route_weight: float32 [3072, 2], P('fs'), may hold values from 0.1 to 1
Outputs:
- gate_out: bfloat16 [8, 4096, 512], P('fs', None, 'tp')
- up_out: bfloat16 [8, 4096, 512], P('fs', None, 'tp')
- down_out: bfloat16 [8, 4096, 512], P('fs', None, 'tp')
- mixed: bfloat16 [3072, 4096], P('fs', 'tp')
Inputs may be any that keep to these rules, and one draw needn't show every extreme that they name: `routes`: within the rows of one index of fs no expert is named by more than 192 pairs, a bound that some block reaches; the 2 experts of a row differ.
All inputs are finite; a program needn't handle non-finite values.
Results may differ from a plain program's by a relative error of at most 0.0087.
Values may be sent and summed in bfloat16 or wider, within the bound.
A program may use at most 128 MiB of HBM per device.

v0:
```python
import jax
import jax.numpy as jnp
from jax import lax
from jax.sharding import PartitionSpec as P

norm_eps = 1e-06


def slot_table(expert_ids, n_experts, capacity, top_count):
    assigned = expert_ids.shape[0]
    onehot = (expert_ids[:, None] == jnp.arange(n_experts, dtype=jnp.int32)[None, :]).astype(
        jnp.int32
    )
    before = jnp.cumsum(onehot, axis=0) - onehot
    slots = jnp.sum(before * onehot, axis=1)
    position = expert_ids * capacity + slots
    owners = jnp.arange(assigned, dtype=jnp.int32) // top_count
    matches = position[None, :] == jnp.arange(n_experts * capacity, dtype=jnp.int32)[:, None]
    slot_token = jnp.max(jnp.where(matches, owners[None, :], -1), axis=1)
    return (position, slot_token)


def place_rows(normed, slot_token):
    padded = jnp.concatenate([normed, jnp.zeros((1, normed.shape[1]), normed.dtype)], axis=0)
    chosen = jnp.where(slot_token < 0, normed.shape[0], slot_token)
    return padded[chosen]


def body(tokens, gate_master, up_master, down_master, norm_gain, routes, route_weight):
    n_experts = gate_master.shape[0]
    tok_rows = routes.shape[0]
    top_count = routes.shape[1]
    capacity = 2 * tok_rows * top_count // n_experts
    folded = norm_gain[None, :, None]
    gate_cast = (gate_master * folded).astype(jnp.bfloat16)
    up_cast = (up_master * folded).astype(jnp.bfloat16)
    down_cast = down_master.astype(jnp.bfloat16)
    gate_out, up_out, down_out = (
        lax.all_to_all(gate_cast, "fs", split_axis=0, concat_axis=1, tiled=True),
        lax.all_to_all(up_cast, "fs", split_axis=0, concat_axis=1, tiled=True),
        lax.all_to_all(down_cast, "fs", split_axis=0, concat_axis=1, tiled=True),
    )
    flat_routes = routes.reshape(-1)
    position, slot_token = slot_table(flat_routes, n_experts, capacity, top_count)
    mix_weights = route_weight / jnp.sum(route_weight, axis=1, keepdims=True)
    gate_mat = gate_out[0]
    up_mat = up_out[0]
    token_float = tokens.astype(jnp.float32)
    full_width = token_float.shape[1] * lax.axis_size("tp")
    sumsquares = lax.psum(jnp.sum(token_float * token_float, axis=1), "tp")
    inverse = lax.rsqrt(sumsquares / full_width + norm_eps)[:, None]
    normed = (token_float * inverse).astype(jnp.bfloat16)
    outgoing = place_rows(normed, slot_token).reshape(n_experts, capacity, normed.shape[1])
    arrived = lax.all_to_all(outgoing, "fs", split_axis=0, concat_axis=0, tiled=True).reshape(
        -1, normed.shape[1]
    )
    segment = lax.all_gather(arrived, "tp", axis=1, tiled=True)
    gate_val = jnp.dot(segment, gate_mat, preferred_element_type=jnp.float32)
    up_val = jnp.dot(segment, up_mat, preferred_element_type=jnp.float32)
    hidden = (jax.nn.silu(gate_val) * up_val).astype(jnp.bfloat16)
    hidden_whole = lax.all_gather(hidden, "tp", axis=1, tiled=True)
    down_quarter = lax.all_to_all(down_out[0], "tp", split_axis=0, concat_axis=1, tiled=True)
    result = lax.dot_general(
        hidden_whole, down_quarter, (((1,), (1,)), ((), ())), preferred_element_type=jnp.float32
    )
    summed = result.astype(jnp.bfloat16)
    returned = lax.all_to_all(
        summed.reshape(-1, capacity, summed.shape[1]), "fs", split_axis=0, concat_axis=0, tiled=True
    )
    flat_back = returned.reshape(-1, summed.shape[1])
    picked = flat_back[position].astype(jnp.float32).reshape(tok_rows, top_count, summed.shape[1])
    mixed = jnp.sum(mix_weights[:, :, None] * picked, axis=1).astype(jnp.bfloat16)
    return (gate_out, up_out, down_out, mixed)


def solution(mesh):
    placed = (
        P("fs", "tp"),
        P(None, "fs", "tp"),
        P(None, "fs", "tp"),
        P(None, "fs", "tp"),
        P("fs"),
        P("fs", None),
        P("fs", None),
    )
    return jax.shard_map(
        body,
        mesh=mesh,
        in_specs=placed,
        out_specs=(P("fs", None, "tp"), P("fs", None, "tp"), P("fs", None, "tp"), P("fs", "tp")),
        check_vma=False,
    )
```

profile of v0, /device:TPU:0, one launch (start us, length us, event | category | flops | bytes accessed | tf_op | source)
XLA Modules:
  0.0 341.4 jit_solution(13418795608480970905)
XLA Ops:
  7.2 0.0 all-gather.3.cloned.1.call-start
  7.2 0.8 copy.28
  8.0 0.1 eq.39
  8.2 0.1 reshape.132
  8.3 1.7 reduce-window.6
  10.1 0.1 slice.12
  10.1 0.1 copy.30
  10.3 0.2 reduce-window.9
  10.4 0.1 copy.31
  10.5 0.1 fusion.4
  10.6 0.7 select_reduce_fusion
  11.4 1.4 fusion.1
  12.7 8.4 %psum.7 = f32[384]{0:T(512)S(1)} all-reduce(f32[384]{0:T(512)S(1)} %fusion.1), channel_id=1, replica_groups=mesh['fs'=8,'tp'=4] {'tp'}, use_global_device_ids=true, to_apply=%region_2.3 | all-reduce | flops 384 | bytes 3072 | tf_op jit(solution)/shard_map/psum | solution.py:50
  21.1 1.3 fusion.2
  22.5 0.1 concatenate.3
  22.5 5.8 %gather_fusion = bf16[1536,1024]{1,0:T(8,128)(2,1)} fusion(bf16[385,1024]{1,0:T(8,128)(2,1)S(1)} %concatenate.3, s32[2048]{0:T(1024)S(1)} %pad_clamp_fusion), kind=kCustom, calls=%fused_computation | custom fusion | bytes 6297600 | tf_op jit(solution)/shard_map/gather | solution.py:26
  28.4 75.4 %all_to_all.65 = bf16[8,192,1024]{2,1,0:T(8,128)(2,1)} all-to-all(bf16[8,192,1024]{2,1,0:T(8,128)(2,1)} %bitcast.30), channel_id=1, replica_groups=mesh['fs'=8,'tp'=4] {'fs'}, dimensions={0} | all-to-all | bytes 6291456 | tf_op jit(solution)/shard_map/all_to_all | solution.py:54
  103.8 0.0 all-gather.3.cloned.1.call-update
  103.8 1.6 copy-done.6
  105.4 3.0 multiply_convert_fusion
  108.3 28.8 %all_to_all.66 = bf16[8,512,128]{2,1,0:T(8,128)(2,1)S(1)} all-to-all(bf16[8,512,128]{2,1,0:T(8,128)(2,1)S(1)} %get-tuple-element.5), channel_id=1, replica_groups=mesh['fs'=8,'tp'=4] {'fs'}, dimensions={0} | all-to-all | bytes 2097152 | tf_op jit(solution)/shard_map/all_to_all | solution.py:39
  137.1 3.6 %all-to-all-start.1 = ((bf16[8,512,128]{2,1,0:T(8,128)(2,1)}), bf16[8,512,128]{2,1,0:T(8,128)(2,1)S(1)}, u32[]{:S(2)}, u32[]{:S(2)}) async-start(bf16[8,512,128]{2,1,0:T(8,128)(2,1)} %get-tuple-element.4), calls=%async_computation.1 | async-start | bytes 2097152 | tf_op jit(solution)/shard_map/all_to_all | solution.py:40
  140.7 2.7 convert_element_type.40
  143.4 41.7 %all-gather.3.cloned.1.call-done = bf16[1536,4096]{1,0:T(8,128)(2,1)} async-done(((bf16[1536,1024]{1,0:T(8,128)(2,1)}), bf16[1536,4096]{1,0:T(8,128)(2,1)}) %all-gather.3.cloned.1.call-update) | async-done | bytes 12582928 | tf_op jit(solution)/shard_map/all_gather | solution.py:57
  185.1 6.4 %fusion.11 = f32[1536,128]{1,0:T(8,128)S(1)} fusion(bf16[1536,4096]{1,0:T(8,128)(2,1)} %all-gather.3.cloned.1.call-done, bf16[4096,128]{1,0:T(8,128)(2,1)S(1)} %bitcast.33), kind=kOutput, calls=%fused_computation.38 | convolution fusion | flops 1610612736 | bytes 14417920 | tf_op jit(solution)/shard_map/dot_general | solution.py:58
  191.5 0.0 copy-start.4
  191.5 5.5 %all-to-all-start.2 = ((bf16[8,512,128]{2,1,0:T(8,128)(2,1)}), bf16[8,512,128]{2,1,0:T(8,128)(2,1)S(1)}, u32[]{:S(2)}, u32[]{:S(2)}) async-start(bf16[8,512,128]{2,1,0:T(8,128)(2,1)} %convert_element_type.40), calls=%async_computation.2 | async-start | bytes 2097152 | tf_op jit(solution)/shard_map/all_to_all | solution.py:41
  197.1 0.0 all-gather.5.cloned.1.call-start
  197.1 7.4 %fusion = bf16[1536,128]{1,0:T(8,128)(2,1)} fusion(bf16[1536,4096]{1,0:T(8,128)(2,1)} %all-gather.3.cloned.1.call-done, bf16[4096,128]{1,0:T(8,128)(2,1)S(1)} %bitcast.35, f32[1536,128]{1,0:T(8,128)S(1)} %fusion.11), kind=kOutput, calls=%fused_computation.7 | convolution fusion | flops 1611792384 | bytes 14811136 | tf_op jit(solution)/shard_map/dot_general | solution.py:59
  204.5 0.0 all-gather.5.cloned.1.call-update
  204.5 18.7 %all-to-all-done.2 = bf16[8,512,128]{2,1,0:T(8,128)(2,1)S(1)} async-done(((bf16[8,512,128]{2,1,0:T(8,128)(2,1)}), bf16[8,512,128]{2,1,0:T(8,128)(2,1)S(1)}, u32[]{:S(2)}, u32[]{:S(2)}) %all-to-all-start.2) | async-done | bytes 1048608 | tf_op jit(solution)/shard_map/all_to_all | solution.py:41
  223.3 16.8 %all_to_all.67 = bf16[4,1024,128]{2,1,0:T(8,128)(2,1)S(1)} all-to-all(bf16[4,1024,128]{2,1,0:T(8,128)(2,1)S(1)} %bitcast.31), channel_id=1, replica_groups=mesh['fs'=8,'tp'=4] {'tp'}, dimensions={0} | all-to-all | bytes 2097152 | tf_op jit(solution)/shard_map/all_to_all | solution.py:62
  240.1 0.5 copy.32
  240.6 0.0 all-gather.5.cloned.1.call-done
  240.7 4.9 %convolution_convert_fusion = bf16[1536,1024]{1,0:T(8,128)(2,1)} fusion(bf16[1536,512]{1,0:T(8,128)(2,1)} %all-gather.5.cloned.1.call-done, bf16[1024,512]{0,1:T(8,128)(2,1)S(1)} %bitcast.39), kind=kOutput, calls=%fused_computation.4 | convolution fusion | flops 1612185600 | bytes 5767168 | tf_op jit(solution)/shard_map/dot_general | solution.py:63
  245.5 4.0 %all-to-all-start.5 = ((bf16[8,192,1024]{2,1,0:T(8,128)(2,1)}), bf16[8,192,1024]{2,1,0:T(8,128)(2,1)S(1)}, u32[]{:S(2)}, u32[]{:S(2)}) async-start(bf16[8,192,1024]{2,1,0:T(8,128)(2,1)} %bitcast.38), calls=%async_computation.5 | async-start | bytes 6291456 | tf_op jit(solution)/shard_map/all_to_all | solution.py:67
  249.5 0.1 copy.33
  249.7 0.2 mul.81
  249.9 0.1 copy.27
  250.1 69.8 %all-to-all-done.5 = bf16[8,192,1024]{2,1,0:T(8,128)(2,1)S(1)} async-done(((bf16[8,192,1024]{2,1,0:T(8,128)(2,1)}), bf16[8,192,1024]{2,1,0:T(8,128)(2,1)S(1)}, u32[]{:S(2)}, u32[]{:S(2)}) %all-to-all-start.5) | async-done | bytes 3145760 | tf_op jit(solution)/shard_map/all_to_all | solution.py:67
  319.9 3.6 %gather_fusion.1 = bf16[768,1024]{1,0:T(8,128)(2,1)} fusion(bf16[1536,1024]{1,0:T(8,128)(2,1)S(1)} %bitcast.28, s32[1024]{0:T(1024)S(1)} %pad_clamp_fusion.1), kind=kCustom, calls=%fused_computation.1 | custom fusion | bytes 3148800 | tf_op jit(solution)/shard_map/gather | solution.py:71
  323.4 3.4 reshape.138
  326.8 0.0 copy-start.3
  326.9 0.0 copy-start.5
  326.9 4.8 %multiply_reduce_fusion = bf16[384,1024]{1,0:T(8,128)(2,1)} fusion(f32[384,2,1024]{2,1,0:T(2,128)S(1)} %reshape.138, f32[384,2]{1,0:T(8,128)S(1)} %copy.27), kind=kLoop, calls=%fused_computation.5 | loop fusion | flops 1179648 | bytes 3935232 | tf_op jit(solution)/shard_map/reduce_sum | solution.py:72
  331.7 1.0 copy.37
  332.7 1.0 copy.38
  333.6 1.0 copy.39
  (27 shorter events, 0.1 us)
Async XLA Ops:
  7.2 177.9 %all-gather.3.cloned.1.call-start = ((), (), s32[]{:S(2)}) async-start(), calls=%async_computation.6 | async-start | bytes 15728640 | tf_op jit(solution)/shard_map/all_gather | solution.py:57
  103.8 1.6 copy-start.6
  103.8 1.6 copy-start.9
  137.1 54.4 %copy-start.2 = (bf16[8,512,128]{2,1,0:T(8,128)(2,1)}, bf16[8,512,128]{2,1,0:T(8,128)(2,1)S(1)}, u32[]{:S(2)}) copy-start(bf16[8,512,128]{2,1,0:T(8,128)(2,1)S(1)} %all_to_all.66) | copy-start | bytes 3145732
  137.1 54.4 %all-to-all-start.1 = ((bf16[8,512,128]{2,1,0:T(8,128)(2,1)}), bf16[8,512,128]{2,1,0:T(8,128)(2,1)S(1)}, u32[]{:S(2)}, u32[]{:S(2)}) async-start(bf16[8,512,128]{2,1,0:T(8,128)(2,1)} %get-tuple-element.4), calls=%async_computation.1 | async-start | bytes 2097152 | tf_op jit(solution)/shard_map/all_to_all | solution.py:40
  191.5 13.0 %copy-start.4 = (bf16[8,512,128]{2,1,0:T(8,128)(2,1)}, bf16[8,512,128]{2,1,0:T(8,128)(2,1)S(1)}, u32[]{:S(2)}) copy-start(bf16[8,512,128]{2,1,0:T(8,128)(2,1)S(1)} %all-to-all-done.1) | copy-start | bytes 3145732
  191.5 31.7 %all-to-all-start.2 = ((bf16[8,512,128]{2,1,0:T(8,128)(2,1)}), bf16[8,512,128]{2,1,0:T(8,128)(2,1)S(1)}, u32[]{:S(2)}, u32[]{:S(2)}) async-start(bf16[8,512,128]{2,1,0:T(8,128)(2,1)} %convert_element_type.40), calls=%async_computation.2 | async-start | bytes 2097152 | tf_op jit(solution)/shard_map/all_to_all | solution.py:41
  197.1 43.6 %all-gather.5.cloned.1.call-start = ((), (), s32[]{:S(2)}) async-start(), calls=%async_computation.7 | async-start | bytes 1966080 | tf_op jit(solution)/shard_map/all_gather | solution.py:61
  223.3 22.3 %copy-start = (bf16[8,512,128]{2,1,0:T(8,128)(2,1)}, bf16[8,512,128]{2,1,0:T(8,128)(2,1)S(1)}, u32[]{:S(2)}) copy-start(bf16[8,512,128]{2,1,0:T(8,128)(2,1)S(1)} %all-to-all-done.2) | copy-start | bytes 3145732
  245.5 4.0 %copy-start.8 = (s32[384,2]{0,1:T(2,128)S(1)}, s32[384,2]{0,1:T(2,128)}, u32[]{:S(2)}) copy-start(s32[384,2]{0,1:T(2,128)} %param.12) | copy-start | bytes 9220
  245.5 4.3 %copy-start.7 = (f32[384,2]{0,1:T(2,128)S(1)}, f32[384,2]{0,1:T(2,128)}, u32[]{:S(2)}) copy-start(f32[384,2]{0,1:T(2,128)} %param.13) | copy-start | bytes 9220
  245.5 74.3 %all-to-all-start.5 = ((bf16[8,192,1024]{2,1,0:T(8,128)(2,1)}), bf16[8,192,1024]{2,1,0:T(8,128)(2,1)S(1)}, u32[]{:S(2)}, u32[]{:S(2)}) async-start(bf16[8,192,1024]{2,1,0:T(8,128)(2,1)} %bitcast.38), calls=%async_computation.5 | async-start | bytes 6291456 | tf_op jit(solution)/shard_map/all_to_all | solution.py:67
  326.8 4.8 %copy-start.3 = (bf16[8,512,128]{2,1,0:T(8,128)(2,1)S(1)}, bf16[8,512,128]{2,1,0:T(8,128)(2,1)}, u32[]{:S(2)}) copy-start(bf16[8,512,128]{2,1,0:T(8,128)(2,1)} %copy-done.2) | copy-start | bytes 3145732
  326.9 5.8 %copy-start.5 = (bf16[8,512,128]{2,1,0:T(8,128)(2,1)S(1)}, bf16[8,512,128]{2,1,0:T(8,128)(2,1)}, u32[]{:S(2)}) copy-start(bf16[8,512,128]{2,1,0:T(8,128)(2,1)} %copy-done.4) | copy-start | bytes 3145732
  326.9 6.8 %copy-start.1 = (bf16[8,512,128]{2,1,0:T(8,128)(2,1)S(1)}, bf16[8,512,128]{2,1,0:T(8,128)(2,1)}, u32[]{:S(2)}) copy-start(bf16[8,512,128]{2,1,0:T(8,128)(2,1)} %copy-done) | copy-start | bytes 3145732
Sparse Core Ops, SparseCore 0:
  103.9 81.1 all-gather.2
  204.6 20.2 all-gather.4
where the time goes:
time: 342 us; the launch traced here: 341 us
  waiting for transfers between devices  130 us (38%)
  blocking collectives  129 us (38%)
  local copies, waits for them, and re-layouts  19.7 us (6%)
  matrix products  18.6 us (5%)
  other arithmetic  16 us (5%)
  between operations  14.3 us (4%)
  starting transfers between devices  13.1 us (4%)
    all_to_all x1, blocking collectives, body(): lax.all_to_all(outgoing, 'fs', split_axis=0, concat_axis=0, tiled=True)  75.4 us
    all_to_all x1, waiting for transfers between devices, body(): lax.all_to_all(summed.reshape(-1, capacity, summed.shape[1]), 'fs', split...  69.8 us
    all_gather x1, waiting for transfers between devices, body(): segment = lax.all_gather(arrived, 'tp', axis=1, tiled=True)  41.7 us
    all_to_all x1, blocking collectives, body(): lax.all_to_all(gate_cast, 'fs', split_axis=0, concat_axis=1, tiled=True)  28.8 us
    all_to_all x1, waiting for transfers between devices, body(): lax.all_to_all(down_cast, 'fs', split_axis=0, concat_axis=1, tiled=True)  18.7 us
    all_to_all x1, blocking collectives, body(): lax.all_to_all(down_out[0], 'tp', split_axis=0, concat_axis=1, tiled=True)  16.8 us
    psum x1, blocking collectives, body(): sumsquares = lax.psum(jnp.sum(token_float * token_float, axis=1), 'tp')  8.39 us
    dot_general x1, matrix products, body(): up_val = jnp.dot(segment, up_mat, preferred_element_type=jnp.float32)  7.37 us
  transfers between devices with their start and end apart: 5, of which 3 were waited for; matrix products, arithmetic and copies ran while one was open for 6% of the time, Pallas kernels for 0%

commit v1 on v0

--- a/solution.py
+++ b/solution.py
@@ -4,6 +4,12 @@
 from jax.sharding import PartitionSpec as P
 
 norm_eps = 1e-06
+
+
+def exchange_blocks(value, axis, split, join):
+    pieces = jnp.split(value, lax.axis_size(axis), axis=split)
+    received = lax.all_to_all(jnp.stack(pieces), axis, 0, 0)
+    return jnp.concatenate(received, axis=join)
 
 
 def slot_table(expert_ids, n_experts, capacity, top_count):
@@ -38,7 +44,7 @@
     gate_out, up_out, down_out = (
         lax.all_to_all(gate_cast, "fs", split_axis=0, concat_axis=1, tiled=True),
         lax.all_to_all(up_cast, "fs", split_axis=0, concat_axis=1, tiled=True),
-        lax.all_to_all(down_cast, "fs", split_axis=0, concat_axis=1, tiled=True),
+        exchange_blocks(down_cast, "fs", 0, 1),
     )
     flat_routes = routes.reshape(-1)
     position, slot_token = slot_table(flat_routes, n_experts, capacity, top_count)

time: 342 us -> 342 us (level)
  blocking collectives: 129 us -> 101 us
  waiting for transfers between devices: 130 us -> 150 us
  local copies, waits for them, and re-layouts: 19.7 us -> 25.1 us
  starting transfers between devices: 13.1 us -> 16.7 us
    all_to_all x1 -> x0, blocking collectives: 28.8 us -> none  [body(): lax.all_to_all(gate_cast, 'fs', split_axis=0, concat_axis=1, tiled=True)]
    all_to_all x1 -> x2, waiting for transfers between devices: 18.7 us -> 38.7 us  [the longest x1 20 us: body(): lax.all_to_all(gate_cast, 'fs', split_axis=0, concat_axis=1, tiled=True)]
    unnamed x24 -> x31, local copies, waits for them, and re-layouts: 5.33 us -> 9.98 us
    all_to_all x1 -> x2, starting transfers between devices: 5.53 us -> 9.11 us  [the longest x1 5.52 us: exchange_blocks(): received = lax.all_to_all(jnp.stack(pieces), axis, 0, 0)]
  transfers between devices with their start and end apart: 5 -> 6, of which waited for: 3 -> 4; matrix products, arithmetic and copies ran while one was open for 6% -> 8% of each run, Pallas kernels for 0% -> 0%
where the time goes in v1:
time: 342 us; the launch traced here: 341 us
  waiting for transfers between devices  150 us (44%)
  blocking collectives  101 us (30%)
  local copies, waits for them, and re-layouts  25.1 us (7%)
  matrix products  18.6 us (5%)
  starting transfers between devices  16.7 us (5%)
  other arithmetic  15.9 us (5%)
  between operations  14.3 us (4%)
    all_to_all x1, blocking collectives, body(): lax.all_to_all(outgoing, 'fs', split_axis=0, concat_axis=0, tiled=True)  75.4 us
    all_to_all x1, waiting for transfers between devices, body(): lax.all_to_all(summed.reshape(-1, capacity, summed.shape[1]), 'fs', split...  69.8 us
    all_gather x1, waiting for transfers between devices, body(): segment = lax.all_gather(arrived, 'tp', axis=1, tiled=True)  41.6 us
    all_to_all x1, waiting for transfers between devices, body(): lax.all_to_all(gate_cast, 'fs', split_axis=0, concat_axis=1, tiled=True)  20 us
    all_to_all x1, waiting for transfers between devices, exchange_blocks(): received = lax.all_to_all(jnp.stack(pieces), axis, 0, 0)  18.7 us
    all_to_all x1, blocking collectives, body(): lax.all_to_all(down_out[0], 'tp', split_axis=0, concat_axis=1, tiled=True)  16.8 us
    unnamed x31, local copies, waits for them, and re-layouts  9.98 us
    psum x1, blocking collectives, body(): sumsquares = lax.psum(jnp.sum(token_float * token_float, axis=1), 'tp')  8.39 us
  transfers between devices with their start and end apart: 6, of which 4 were waited for; matrix products, arithmetic and copies ran while one was open for 8% of the time, Pallas kernels for 0%

profile of v1, /device:TPU:0, one launch (start us, length us, event | category | flops | bytes accessed | tf_op | source)
XLA Modules:
  0.0 341.4 jit_solution(10141146430103839362)
XLA Ops:
  7.2 0.8 copy.42
  8.0 0.1 eq.39
  8.2 0.1 reshape.132
  8.3 1.7 reduce-window.6
  10.1 0.1 slice.12
  10.1 0.1 copy.44
  10.3 0.2 reduce-window.9
  10.4 0.1 copy.45
  10.5 0.1 fusion.12
  10.6 0.7 select_reduce_fusion
  11.4 1.4 fusion.1
  12.7 8.4 %psum.7 = f32[384]{0:T(512)S(1)} all-reduce(f32[384]{0:T(512)S(1)} %fusion.1), channel_id=1, replica_groups=mesh['fs'=8,'tp'=4] {'tp'}, use_global_device_ids=true, to_apply=%region_2.3 | all-reduce | flops 384 | bytes 3072 | tf_op jit(solution)/shard_map/psum | solution.py:56
  21.1 1.3 fusion.2
  22.5 5.8 %gather_fusion = bf16[1536,1024]{1,0:T(8,128)(2,1)} fusion(bf16[385,1024]{1,0:T(8,128)(2,1)S(1)} %concatenate.3, s32[2048]{0:T(1024)S(1)} %pad_clamp_fusion), kind=kCustom, calls=%fused_computation | custom fusion | bytes 6297600 | tf_op jit(solution)/shard_map/gather | solution.py:32
  28.4 75.4 %all_to_all.58 = bf16[8,192,1024]{2,1,0:T(8,128)(2,1)} all-to-all(bf16[8,192,1024]{2,1,0:T(8,128)(2,1)} %bitcast.62), channel_id=1, replica_groups=mesh['fs'=8,'tp'=4] {'fs'}, dimensions={0} | all-to-all | bytes 6291456 | tf_op jit(solution)/shard_map/all_to_all | solution.py:60
  103.8 1.6 copy-done.6
  105.4 3.5 %multiply_convert_fusion = (bf16[8,512,128]{2,1,0:T(8,128)(2,1)}, bf16[8,512,128]{2,1,0:T(8,128)(2,1)}) fusion(f32[8,512,128]{2,1,0:T(8,128)S(1)} %copy-done.6, f32[512]{0:T(512)S(1)} %copy-done.9, f32[8,512,128]{2,1,0:T(8,128)} %param.8), kind=kLoop, calls=%fused_computation.8 | loop fusion | flops 2097152 | bytes 6293504 | tf_op jit(solution)/shard_map/convert_element_type | solution.py:42
  108.8 3.6 %all-to-all-start = ((bf16[8,512,128]{2,1,0:T(8,128)(2,1)}), bf16[8,512,128]{2,1,0:T(8,128)(2,1)S(1)}, u32[]{:S(2)}, u32[]{:S(2)}) async-start(bf16[8,512,128]{2,1,0:T(8,128)(2,1)} %get-tuple-element.5), calls=%async_computation | async-start | bytes 2097152 | tf_op jit(solution)/shard_map/all_to_all | solution.py:45
  112.4 2.2 convert_element_type.40
  114.6 0.7 fusion.10
  115.3 0.7 fusion.9
  116.0 0.7 fusion.8
  116.6 0.7 fusion.7
  117.3 0.7 fusion.6
  117.9 20.0 %all-to-all-done = bf16[8,512,128]{2,1,0:T(8,128)(2,1)S(1)} async-done(((bf16[8,512,128]{2,1,0:T(8,128)(2,1)}), bf16[8,512,128]{2,1,0:T(8,128)(2,1)S(1)}, u32[]{:S(2)}, u32[]{:S(2)}) %all-to-all-start) | async-done | bytes 1048608 | tf_op jit(solution)/shard_map/all_to_all | solution.py:45
  137.9 3.6 %all-to-all-start.1 = ((bf16[8,512,128]{2,1,0:T(8,128)(2,1)}), bf16[8,512,128]{2,1,0:T(8,128)(2,1)S(1)}, u32[]{:S(2)}, u32[]{:S(2)}) async-start(bf16[8,512,128]{2,1,0:T(8,128)(2,1)} %get-tuple-element.4), calls=%async_computation.1 | async-start | bytes 2097152 | tf_op jit(solution)/shard_map/all_to_all | solution.py:46
  141.5 0.7 fusion.5
  142.2 0.7 fusion.4
  142.8 0.7 fusion.3
  143.5 41.6 %all-gather.3.cloned.1.call-done = bf16[1536,4096]{1,0:T(8,128)(2,1)} async-done(((bf16[1536,1024]{1,0:T(8,128)(2,1)}), bf16[1536,4096]{1,0:T(8,128)(2,1)}) %all-gather.3.cloned.1.call-update) | async-done | bytes 12582928 | tf_op jit(solution)/shard_map/all_gather | solution.py:63
  185.1 6.4 %fusion.19 = f32[1536,128]{1,0:T(8,128)S(1)} fusion(bf16[1536,4096]{1,0:T(8,128)(2,1)} %all-gather.3.cloned.1.call-done, bf16[4096,128]{1,0:T(8,128)(2,1)S(1)} %bitcast.65), kind=kOutput, calls=%fused_computation.54 | convolution fusion | flops 1610612736 | bytes 14417920 | tf_op jit(solution)/shard_map/dot_general | solution.py:64
  191.5 5.5 %all-to-all-start.2 = ((bf16[8,1,512,128]{3,2,1,0:T(8,128)(2,1)}), bf16[8,1,512,128]{3,2,1,0:T(8,128)(2,1)S(1)}, u32[]{:S(2)}, u32[]{:S(2)}) async-start(bf16[8,1,512,128]{3,2,1,0:T(8,128)(2,1)} %fusion.3), calls=%async_computation.2 | async-start | bytes 2097152 | tf_op jit(solution)/shard_map/all_to_all | solution.py:11
  197.1 7.4 %fusion = bf16[1536,128]{1,0:T(8,128)(2,1)} fusion(bf16[1536,4096]{1,0:T(8,128)(2,1)} %all-gather.3.cloned.1.call-done, bf16[4096,128]{1,0:T(8,128)(2,1)S(1)} %bitcast.67, f32[1536,128]{1,0:T(8,128)S(1)} %fusion.19), kind=kOutput, calls=%fused_computation.7 | convolution fusion | flops 1611792384 | bytes 14811136 | tf_op jit(solution)/shard_map/dot_general | solution.py:65
  204.5 18.7 %all-to-all-done.2 = bf16[8,1,512,128]{3,2,1,0:T(8,128)(2,1)S(1)} async-done(((bf16[8,1,512,128]{3,2,1,0:T(8,128)(2,1)}), bf16[8,1,512,128]{3,2,1,0:T(8,128)(2,1)S(1)}, u32[]{:S(2)}, u32[]{:S(2)}) %all-to-all-start.2) | async-done | bytes 1048608 | tf_op jit(solution)/shard_map/all_to_all | solution.py:11
  223.3 16.8 %all_to_all.59 = bf16[4,1024,128]{2,1,0:T(8,128)(2,1)S(1)} all-to-all(bf16[4,1024,128]{2,1,0:T(8,128)(2,1)S(1)} %bitcast.63), channel_id=1, replica_groups=mesh['fs'=8,'tp'=4] {'tp'}, dimensions={0} | all-to-all | bytes 2097152 | tf_op jit(solution)/shard_map/all_to_all | solution.py:68
  240.1 0.5 copy.46
  240.7 4.9 %convolution_convert_fusion = bf16[1536,1024]{1,0:T(8,128)(2,1)} fusion(bf16[1536,512]{1,0:T(8,128)(2,1)} %all-gather.5.cloned.1.call-done, bf16[1024,512]{0,1:T(8,128)(2,1)S(1)} %bitcast.71), kind=kOutput, calls=%fused_computation.4 | convolution fusion | flops 1612185600 | bytes 5767168 | tf_op jit(solution)/shard_map/dot_general | solution.py:69
  245.5 4.0 %all-to-all-start.5 = ((bf16[8,192,1024]{2,1,0:T(8,128)(2,1)}), bf16[8,192,1024]{2,1,0:T(8,128)(2,1)S(1)}, u32[]{:S(2)}, u32[]{:S(2)}) async-start(bf16[8,192,1024]{2,1,0:T(8,128)(2,1)} %bitcast.70), calls=%async_computation.5 | async-start | bytes 6291456 | tf_op jit(solution)/shard_map/all_to_all | solution.py:73
  249.5 0.1 copy.47
  249.7 0.2 mul.81
  249.9 0.1 copy.41
  250.1 69.8 %all-to-all-done.5 = bf16[8,192,1024]{2,1,0:T(8,128)(2,1)S(1)} async-done(((bf16[8,192,1024]{2,1,0:T(8,128)(2,1)}), bf16[8,192,1024]{2,1,0:T(8,128)(2,1)S(1)}, u32[]{:S(2)}, u32[]{:S(2)}) %all-to-all-start.5) | async-done | bytes 3145760 | tf_op jit(solution)/shard_map/all_to_all | solution.py:73
  319.9 3.6 %gather_fusion.1 = bf16[768,1024]{1,0:T(8,128)(2,1)} fusion(bf16[1536,1024]{1,0:T(8,128)(2,1)S(1)} %bitcast.60, s32[1024]{0:T(1024)S(1)} %pad_clamp_fusion.1), kind=kCustom, calls=%fused_computation.1 | custom fusion | bytes 3148800 | tf_op jit(solution)/shard_map/gather | solution.py:77
  323.4 3.4 reshape.138
  326.9 4.8 %multiply_reduce_fusion = bf16[384,1024]{1,0:T(8,128)(2,1)} fusion(f32[384,2,1024]{2,1,0:T(2,128)S(1)} %reshape.138, f32[384,2]{1,0:T(8,128)S(1)} %copy.41), kind=kLoop, calls=%fused_computation.5 | loop fusion | flops 1179648 | bytes 3935232 | tf_op jit(solution)/shard_map/reduce_sum | solution.py:78
  331.7 1.0 copy.58
  332.7 1.0 copy.59
  333.6 1.0 copy.60
  (36 shorter events, 0.3 us)
Async XLA Ops:
  7.2 177.9 %all-gather.3.cloned.1.call-start = ((), (), s32[]{:S(2)}) async-start(), calls=%async_computation.6 | async-start | bytes 15728640 | tf_op jit(solution)/shard_map/all_gather | solution.py:63
  103.8 1.6 copy-start.6
  103.8 1.6 copy-start.9
  108.8 29.1 %all-to-all-start = ((bf16[8,512,128]{2,1,0:T(8,128)(2,1)}), bf16[8,512,128]{2,1,0:T(8,128)(2,1)S(1)}, u32[]{:S(2)}, u32[]{:S(2)}) async-start(bf16[8,512,128]{2,1,0:T(8,128)(2,1)} %get-tuple-element.5), calls=%async_computation | async-start | bytes 2097152 | tf_op jit(solution)/shard_map/all_to_all | solution.py:45
  137.9 53.6 %copy-start.2 = (bf16[8,512,128]{2,1,0:T(8,128)(2,1)}, bf16[8,512,128]{2,1,0:T(8,128)(2,1)S(1)}, u32[]{:S(2)}) copy-start(bf16[8,512,128]{2,1,0:T(8,128)(2,1)S(1)} %all-to-all-done) | copy-start | bytes 3145732
  137.9 53.6 %all-to-all-start.1 = ((bf16[8,512,128]{2,1,0:T(8,128)(2,1)}), bf16[8,512,128]{2,1,0:T(8,128)(2,1)S(1)}, u32[]{:S(2)}, u32[]{:S(2)}) async-start(bf16[8,512,128]{2,1,0:T(8,128)(2,1)} %get-tuple-element.4), calls=%async_computation.1 | async-start | bytes 2097152 | tf_op jit(solution)/shard_map/all_to_all | solution.py:46
  191.5 12.9 %copy-start.4 = (bf16[8,512,128]{2,1,0:T(8,128)(2,1)}, bf16[8,512,128]{2,1,0:T(8,128)(2,1)S(1)}, u32[]{:S(2)}) copy-start(bf16[8,512,128]{2,1,0:T(8,128)(2,1)S(1)} %all-to-all-done.1) | copy-start | bytes 3145732
  191.5 31.7 %all-to-all-start.2 = ((bf16[8,1,512,128]{3,2,1,0:T(8,128)(2,1)}), bf16[8,1,512,128]{3,2,1,0:T(8,128)(2,1)S(1)}, u32[]{:S(2)}, u32[]{:S(2)}) async-start(bf16[8,1,512,128]{3,2,1,0:T(8,128)(2,1)} %fusion.3), calls=%async_computation.2 | async-start | bytes 2097152 | tf_op jit(solution)/shard_map/all_to_all | solution.py:11
  197.1 43.6 %all-gather.5.cloned.1.call-start = ((), (), s32[]{:S(2)}) async-start(), calls=%async_computation.7 | async-start | bytes 1966080 | tf_op jit(solution)/shard_map/all_gather | solution.py:67
  223.3 22.3 %copy-start = (bf16[8,1,512,128]{3,2,1,0:T(8,128)(2,1)}, bf16[8,1,512,128]{3,2,1,0:T(8,128)(2,1)S(1)}, u32[]{:S(2)}) copy-start(bf16[8,1,512,128]{3,2,1,0:T(8,128)(2,1)S(1)} %all-to-all-done.2) | copy-start | bytes 3145732
  245.5 4.0 %copy-start.8 = (s32[384,2]{0,1:T(2,128)S(1)}, s32[384,2]{0,1:T(2,128)}, u32[]{:S(2)}) copy-start(s32[384,2]{0,1:T(2,128)} %param.12) | copy-start | bytes 9220
  245.5 4.3 %copy-start.7 = (f32[384,2]{0,1:T(2,128)S(1)}, f32[384,2]{0,1:T(2,128)}, u32[]{:S(2)}) copy-start(f32[384,2]{0,1:T(2,128)} %param.13) | copy-start | bytes 9220
  245.5 74.3 %all-to-all-start.5 = ((bf16[8,192,1024]{2,1,0:T(8,128)(2,1)}), bf16[8,192,1024]{2,1,0:T(8,128)(2,1)S(1)}, u32[]{:S(2)}, u32[]{:S(2)}) async-start(bf16[8,192,1024]{2,1,0:T(8,128)(2,1)} %bitcast.70), calls=%async_computation.5 | async-start | bytes 6291456 | tf_op jit(solution)/shard_map/all_to_all | solution.py:73
  326.8 4.8 %copy-start.3 = (bf16[8,512,128]{2,1,0:T(8,128)(2,1)S(1)}, bf16[8,512,128]{2,1,0:T(8,128)(2,1)}, u32[]{:S(2)}) copy-start(bf16[8,512,128]{2,1,0:T(8,128)(2,1)} %copy-done.2) | copy-start | bytes 3145732
  326.9 5.8 %copy-start.5 = (bf16[8,512,128]{2,1,0:T(8,128)(2,1)S(1)}, bf16[8,512,128]{2,1,0:T(8,128)(2,1)}, u32[]{:S(2)}) copy-start(bf16[8,512,128]{2,1,0:T(8,128)(2,1)} %copy-done.4) | copy-start | bytes 3145732
  326.9 6.8 %copy-start.1 = (bf16[8,1,512,128]{3,2,1,0:T(8,128)(2,1)S(1)}, bf16[8,1,512,128]{3,2,1,0:T(8,128)(2,1)}, u32[]{:S(2)}) copy-start(bf16[8,1,512,128]{3,2,1,0:T(8,128)(2,1)} %copy-done) | copy-start | bytes 3145732
Sparse Core Ops, SparseCore 0:
  103.9 81.1 all-gather.2
  204.6 20.2 all-gather.4
